TPU v7x, 32 devices: a whole 2x2x4 slice. The times are simulated.
32 devices in a mesh: kv: 8 (over z, y), tp: 4 (over x, core).
Axes of the slice: x: 2, y: 2, z: 4, core: 2. Of those that a mesh axis runs over, the one named last changes fastest.
Arguments:
- tokens: bfloat16 [16, 4096], P(None, 'tp'), may hold values from -6 to 6
- norm_gain: float32 [4096], P('tp'), may hold values from 0.1 to 1.9
- w_query: bfloat16 [4096, 32, 96], P('tp', 'kv'), as said below
- w_latent: bfloat16 [4096, 1024], P('tp', 'kv'), may hold values from -0.09375 to 0.09375
- w_rotary: bfloat16 [4096, 32], P('tp'), may hold values from -0.09375 to 0.09375
- latent_gain: float32 [1024], replicated, may hold values from 0.1 to 1.9
- w_key_up: bfloat16 [1024, 32, 64], P('tp', 'kv'), may hold values from -0.1875 to 0.1875
- w_value_up: bfloat16 [1024, 32, 128], replicated, may hold values from -0.1875 to 0.1875
- w_out: bfloat16 [4096, 4096], P('kv', 'tp'), may hold values from -0.09375 to 0.09375
- cache_latent: bfloat16 [16, 4096, 1024], P(None, ('kv', 'tp')), may hold values from -6 to 6
- cache_rotary: bfloat16 [16, 4096, 32], P(None, ('kv', 'tp')), may hold values from -6 to 6
- lengths: int32 [16], replicated, may hold values from 1024 to 4096
Outputs:
- mixed_out: bfloat16 [16, 4096], P(None, 'tp')
- new_latent: bfloat16 [16, 1024], P(None, ('kv', 'tp'))
- new_rotary: bfloat16 [16, 32], replicated
Inputs may be any that keep to these rules, and one draw needn't show every extreme that they name: `w_query`: finite.
All inputs are finite; a program needn't handle non-finite values.
Results may differ from a plain program's by a relative error of at most 0.012.
The roundings to bfloat16 on the way count: a program that leaves them out, or rounds other values in their place, can miss the bound.
Values may be sent and summed in bfloat16 or wider, within the bound.
A program may use at most 64 MiB of HBM per device.

v0:
```python
import jax
import jax.numpy as jnp
from jax import lax
from jax.sharding import PartitionSpec as P

THETA = 10000.0
EPS = 1e-06


def rotate(values, position):
    full_width = values.shape[-1]
    half_width = full_width // 2
    frequency = THETA ** (-jnp.arange(0, full_width, 2, dtype=jnp.float32) / full_width)
    angles = position.astype(jnp.float32)[:, None] * frequency[None, :]
    angles = angles.reshape((angles.shape[0],) + (1,) * (values.ndim - 2) + (half_width,))
    cosine = jnp.cos(angles)
    sine_part = jnp.sin(angles)
    first_half = values[..., :half_width]
    second_half = values[..., half_width:]
    return jnp.concatenate(
        [
            first_half * cosine - second_half * sine_part,
            first_half * sine_part + second_half * cosine,
        ],
        axis=-1,
    )


def value_product(latent_f, weight):
    high_part = latent_f.astype(jnp.bfloat16)
    low_part = (latent_f - high_part.astype(jnp.float32)).astype(jnp.bfloat16)
    return jnp.einsum(
        "bhr,rhv->bhv", high_part, weight, preferred_element_type=jnp.float32
    ) + jnp.einsum("bhr,rhv->bhv", low_part, weight, preferred_element_type=jnp.float32)


def shards(
    tokens,
    norm_gain,
    w_query,
    w_latent,
    w_rotary,
    latent_gain,
    w_key_up,
    w_value_up,
    w_out,
    cache_latent,
    cache_rotary,
    lengths,
):
    seq_count = tokens.shape[0]
    kv_count = lax.axis_size("kv")
    tp_count = lax.axis_size("tp")
    kv_index = lax.axis_index("kv")
    tp_index = lax.axis_index("tp")
    heads_dev = w_query.shape[1]
    head_count = heads_dev * kv_count
    latent_rank = cache_latent.shape[2]
    rope_width = cache_rotary.shape[2]
    nope_width = w_query.shape[2] - rope_width
    model_width = tokens.shape[1] * tp_count
    score_scale = w_query.shape[2] ** (-0.5)
    tokens_f = tokens.astype(jnp.float32)
    scaled = (tokens_f * norm_gain).astype(jnp.bfloat16)
    query_part = jnp.einsum("bd,dhn->bhn", scaled, w_query, preferred_element_type=jnp.float32)
    latent_part = jnp.dot(scaled, w_latent, preferred_element_type=jnp.float32)
    rotary_part = jnp.dot(scaled, w_rotary, preferred_element_type=jnp.float32)
    square_part = jnp.sum(tokens_f * tokens_f, axis=1)
    query_sum, latent_sum, rotary_sum, square_sum = lax.psum(
        (query_part, latent_part, rotary_part, square_part), "tp"
    )
    inverse = lax.rsqrt(square_sum / model_width + EPS)
    query_heads = (query_sum * inverse[:, None, None]).astype(jnp.bfloat16)
    compressed = (latent_sum * inverse[:, None]).astype(jnp.bfloat16)
    new_rotary = rotate(rotary_sum * inverse[:, None], lengths).astype(jnp.bfloat16)
    query_rope = rotate(query_heads[:, :, nope_width:].astype(jnp.float32), lengths).astype(
        jnp.bfloat16
    )
    query_latent = jnp.einsum(
        "bhn,rhn->bhr", query_heads[:, :, :nope_width], w_key_up, preferred_element_type=jnp.float32
    ).astype(jnp.bfloat16)
    rope_slice = rope_width // tp_count
    column_slice = compressed.shape[1] // tp_count
    rope_piece = lax.dynamic_slice_in_dim(query_rope, tp_index * rope_slice, rope_slice, 2)
    column_piece = lax.dynamic_slice_in_dim(compressed, tp_index * column_slice, column_slice, 1)
    got_latent, got_rope, got_columns = (
        lax.all_gather(query_latent[:, None], ("kv", "tp"), axis=1, tiled=True),
        lax.all_gather(rope_piece[:, None], ("kv", "tp"), axis=1, tiled=True),
        lax.all_gather(column_piece[:, None], ("kv", "tp"), axis=1, tiled=True),
    )
    rank_slice = query_latent.shape[2]
    all_latent = got_latent.reshape(seq_count, kv_count, tp_count, heads_dev, rank_slice)
    all_latent = all_latent.transpose(0, 1, 3, 2, 4).reshape(seq_count, head_count, latent_rank)
    all_rope = got_rope.reshape(seq_count, kv_count, tp_count, heads_dev, rope_slice)
    all_rope = all_rope.transpose(0, 1, 3, 2, 4).reshape(seq_count, head_count, rope_width)
    fresh_f = got_columns.reshape(seq_count, latent_rank).astype(jnp.float32)
    new_latent = (
        fresh_f * lax.rsqrt(jnp.mean(fresh_f * fresh_f, axis=1, keepdims=True) + EPS) * latent_gain
    ).astype(jnp.bfloat16)
    new_latent_f = new_latent.astype(jnp.float32)
    own_score = (
        jnp.einsum("bhr,br->bh", all_latent, new_latent, preferred_element_type=jnp.float32)
        + jnp.einsum("bhq,bq->bh", all_rope, new_rotary, preferred_element_type=jnp.float32)
    ) * score_scale
    pos_dev = cache_latent.shape[1]
    first_pos = (kv_index * tp_count + tp_index) * pos_dev
    position = first_pos + jnp.arange(pos_dev, dtype=jnp.int32)
    valid = position[None, :] < lengths[:, None]
    scores = (
        jnp.einsum("bhr,bpr->bhp", all_latent, cache_latent, preferred_element_type=jnp.float32)
        + jnp.einsum("bhq,bpq->bhp", all_rope, cache_rotary, preferred_element_type=jnp.float32)
    ) * score_scale
    masked = jnp.where(valid[:, None, :], scores, -jnp.inf)
    local_top = jnp.maximum(jnp.max(masked, axis=2), own_score)
    top_score = lax.pmax(local_top, ("kv", "tp"))
    weights = jnp.where(valid[:, None, :], jnp.exp(scores - top_score[:, :, None]), 0.0)
    total_part = jnp.sum(weights, axis=2)
    summed_part = jnp.einsum(
        "bhp,bpr->bhr",
        weights.astype(jnp.bfloat16),
        cache_latent,
        preferred_element_type=jnp.float32,
    )
    own_weight = jnp.exp(own_score - top_score)
    block_own = lax.dynamic_slice_in_dim(own_weight, kv_index * heads_dev, heads_dev, 1)
    value_block_weight = lax.dynamic_slice_in_dim(w_value_up, kv_index * heads_dev, heads_dev, 1)
    totals, summed = lax.psum((total_part, summed_part), ("kv", "tp"))
    block_sum = lax.dynamic_slice_in_dim(summed, kv_index * heads_dev, heads_dev, 1)
    block_total = lax.dynamic_slice_in_dim(totals, kv_index * heads_dev, heads_dev, 1)
    latent_out = (block_sum + block_own[:, :, None] * new_latent_f[:, None, :]) / (
        block_total + block_own
    )[:, :, None]
    head_out = value_product(latent_out, value_block_weight).astype(jnp.bfloat16)
    out_part = jnp.dot(head_out.reshape(seq_count, -1), w_out, preferred_element_type=jnp.float32)
    mixed_out = lax.psum(out_part, "kv").astype(jnp.bfloat16)
    latent_width = latent_rank // (kv_count * tp_count)
    latent_piece = lax.dynamic_slice_in_dim(
        new_latent, (kv_index * tp_count + tp_index) * latent_width, latent_width, 1
    )
    return (mixed_out, latent_piece, new_rotary)


def solution(mesh):
    placed = (
        P(None, "tp"),
        P("tp"),
        P("tp", "kv", None),
        P("tp", "kv"),
        P("tp", None),
        P(),
        P("tp", "kv", None),
        P(),
        P("kv", "tp"),
        P(None, ("kv", "tp"), None),
        P(None, ("kv", "tp"), None),
        P(),
    )
    return jax.shard_map(
        shards,
        mesh=mesh,
        in_specs=placed,
        out_specs=(P(None, "tp"), P(None, ("kv", "tp")), P()),
        check_vma=False,
    )
```

profile of v0, /device:TPU:0, one launch (start us, length us, event | category | flops | bytes accessed | tf_op | source)
XLA Modules:
  0.0 341.0 jit_solution(9099277364081239508)
XLA Ops:
  7.2 0.0 all-gather.6.cloned.1.call-start
  7.2 1.0 fusion.15
  8.2 1.5 fusion.20
  9.7 1.0 fusion.22
  10.7 1.1 fusion.24
  11.9 13.4 %all-reduce = (f32[16,4,96]{2,0,1:T(8,128)S(1)}, f32[16]{0:T(128)S(1)}, f32[16,128]{1,0:T(8,128)S(1)}, f32[16,32]{1,0:T(8,128)S(1)}) all-reduce(f32[16,4,96]{2,0,1:T(8,128)S(1)} %fusion.20, f32[16]{0:T(128)S(1)} %fusion.15, f32[16,128]{1,0:T(8,128)S(1)} %fusion.24, f32[16,32]{1,0:T(8,128)S(1)} %fusion.22), channel_id=1, replica_groups=mesh['kv'=8,'tp'=4] {'tp'}, use_global_device_ids=true, to_apply=%region_0.0 | all-reduce | flops 8720 | bytes 69760 | tf_op jit(solution)/shard_map/psum | solution.py:69
  25.3 0.1 multiply_convert_fusion.1
  25.3 1.7 fusion.1
  27.0 0.0 all-gather.6.cloned.1.call-update
  27.0 0.0 all-reduce.3.cloned.1.call-start
  27.1 0.7 convert_element_type.81
  27.8 0.1 broadcast_multiply_fusion
  27.8 0.1 subtract_convert_fusion.3
  28.0 0.1 slice_convert_fusion
  28.0 0.1 subtract_convert_fusion.2
  28.1 0.1 dynamic-slice_maximum_fusion
  28.2 0.1 copy.48
  28.3 41.5 %all-gather.1 = bf16[16,128,8]{0,2,1:T(8,128)(2,1)S(1)} all-gather(bf16[16,4,8]{0,2,1:T(8,128)(2,1)S(1)} %copy.48), channel_id=3, replica_groups=mesh['kv'=8,'tp'=4] {'kv','tp'}, dimensions={1}, use_global_device_ids=true | all-gather | bytes 33792 | tf_op jit(solution)/shard_map/all_gather | solution.py:88
  69.8 0.3 copy.50
  70.1 37.0 %all-gather.3 = bf16[32,32,16]{1,2,0:T(8,128)(2,1)S(1)} all-gather(bf16[1,32,16]{1,2,0:T(8,128)(2,1)S(1)} %get-tuple-element.20), channel_id=4, replica_groups=mesh['kv'=8,'tp'=4] {'kv','tp'}, dimensions={0}, use_global_device_ids=true | all-gather | bytes 33792 | tf_op jit(solution)/shard_map/all_gather | solution.py:89
  107.1 0.1 reshape.167
  107.3 0.1 fusion.54
  107.3 0.1 multiply_reduce_fusion
  107.5 0.7 broadcast_compare_fusion
  108.2 0.2 fusion.33
  108.4 0.1 bitcast_convert_fusion
  108.5 0.0 all-gather.6.cloned.1.call-done
  108.5 2.0 copy.75
  110.6 0.8 reshape.151
  111.3 3.7 %fusion.41 = f32[16,32,128]{2,1,0:T(8,128)S(1)} fusion(bf16[16,32,1024]{2,1,0:T(8,128)(2,1)S(1)} %reshape.151, bf16[16,128,1024]{2,1,0:T(8,128)(2,1)} %param.21), kind=kOutput, calls=%fused_computation.71 | convolution fusion | flops 134217728 | bytes 5505024 | tf_op jit(solution)/shard_map/bhr,bpr->bhp/dot_general | solution.py:110
  115.0 0.4 fusion.16
  115.4 0.3 select_reduce_fusion
  115.7 37.0 %pmax.7 = f32[16,32]{1,0:T(8,128)S(1)} all-reduce(f32[16,32]{1,0:T(8,128)S(1)} %get-tuple-element.11), channel_id=1, replica_groups=mesh['kv'=8,'tp'=4] {'kv','tp'}, use_global_device_ids=true, to_apply=%region_7.8 | all-reduce | flops 512 | bytes 4096 | tf_op jit(solution)/shard_map/pmax | solution.py:115
  152.7 2.9 fusion.9
  155.6 2.5 copy.52
  158.2 0.7 pad_maximum_fusion
  158.9 0.7 dynamic-slice_bitcast_fusion
  159.5 2.1 constant_dynamic-slice_fusion
  161.7 0.3 fusion.7
  161.9 42.7 %psum.54 = f32[16,32]{1,0:T(8,128)S(1)} all-reduce(f32[16,32]{1,0:T(8,128)S(1)} %fusion.7), channel_id=1, replica_groups=mesh['kv'=8,'tp'=4] {'kv','tp'}, use_global_device_ids=true, to_apply=%region_10.11 | all-reduce | flops 512 | bytes 4096 | tf_op jit(solution)/shard_map/psum | solution.py:127
  204.6 0.1 dynamic-slice_add_fusion
  204.7 0.1 copy.53
  204.8 0.1 copy.54
  204.8 89.8 %all-reduce.3.cloned.1.call-done = f32[16,32,1024]{2,0,1:T(8,128)} async-done(((f32[16,32,1024]{2,0,1:T(8,128)}), f32[16,32,1024]{2,0,1:T(8,128)}) %all-reduce.3.cloned.1.call-update) | async-done | bytes 2097168 | tf_op jit(solution)/shard_map/psum | solution.py:127
  294.6 1.3 fusion.4
  295.9 1.3 fusion.3
  297.2 0.3 fusion.27
  297.4 36.8 %psum.55 = bf16[16,1024]{1,0:T(8,128)(2,1)} all-reduce(f32[16,1024]{1,0:T(8,128)S(1)} %fusion.27), channel_id=1, replica_groups=mesh['kv'=8,'tp'=4] {'kv'}, use_global_device_ids=true, to_apply=%region_11.12 | all-reduce | flops 16384 | bytes 98304 | tf_op jit(solution)/shard_map/psum | solution.py:135
  (14 shorter events, 0.1 us)
Async XLA Ops:
  7.2 290.0 %copy-start = (bf16[512,1024]{1,0:T(8,128)(2,1)S(1)}, bf16[512,1024]{1,0:T(8,128)(2,1)}, u32[]{:S(2)}) copy-start(bf16[512,1024]{1,0:T(8,128)(2,1)} %param.20) | copy-start | bytes 3145732
  7.2 101.2 %copy-start.2 = (f32[1024]{0:T(1024)S(1)}, f32[1024]{0:T(1024)}, u32[]{:S(2)}) copy-start(f32[1024]{0:T(1024)} %param.17) | copy-start | bytes 12292
  7.2 101.3 %all-gather.6.cloned.1.call-start = ((), (), s32[]{:S(2)}) async-start(), calls=%async_computation.1 | async-start | bytes 1081344 | tf_op jit(solution)/shard_map/all_gather | solution.py:87
  27.0 267.6 %all-reduce.3.cloned.1.call-start = ((), (), s32[]{:S(2)}) async-start(), calls=%async_computation | async-start | bytes 4194304 | tf_op jit(solution)/shard_map/psum | solution.py:127
  110.5 4.9 %copy-start.1 = (bf16[16,128,32]{1,2,0:T(8,128)(2,1)S(1)}, bf16[16,128,32]{1,2,0:T(8,128)(2,1)}, u32[]{:S(2)}) copy-start(bf16[16,128,32]{1,2,0:T(8,128)(2,1)} %param.22) | copy-start | bytes 393220
Sparse Core Ops, SparseCore 0:
  27.1 54.0 all-gather.5
  158.3 136.2 all-reduce.2
where the time goes:
time: 342 us; the launch traced here: 341 us
  blocking collectives  208 us (61%)
  waiting for transfers between devices  89.9 us (26%)
  matrix products  15.6 us (5%)
  between operations  14.2 us (4%)
  local copies, waits for them, and re-layouts  8.86 us (3%)
  other arithmetic  4.22 us (1%)
    psum x1, waiting for transfers between devices, shards(): totals, summed = lax.psum((total_part, summed_part), ('kv', 'tp'))  89.8 us
    psum x1, blocking collectives, shards(): totals, summed = lax.psum((total_part, summed_part), ('kv', 'tp'))  42.7 us
    all_gather x1, blocking collectives, shards(): lax.all_gather(rope_piece[:, None], ('kv', 'tp'), axis=1, tiled=True)  41.5 us
    all_gather x1, blocking collectives, shards(): lax.all_gather(column_piece[:, None], ('kv', 'tp'), axis=1, tiled=True)  37 us
    pmax x1, blocking collectives, shards(): top_score = lax.pmax(local_top, ('kv', 'tp'))  37 us
    psum x1, blocking collectives, shards(): mixed_out = lax.psum(out_part, 'kv').astype(jnp.bfloat16)  36.8 us
    psum x1, blocking collectives, shards(): lax.psum((query_part, latent_part, rotary_part, square_part), 'tp')  13.4 us
  transfers between devices with their start and end apart: 2, of which 1 were waited for; matrix products, arithmetic and copies ran while one was open for 2% of the time, Pallas kernels for 0%

commit v1 on v0

--- a/solution.py
+++ b/solution.py
@@ -124,7 +124,7 @@
     own_weight = jnp.exp(own_score - top_score)
     block_own = lax.dynamic_slice_in_dim(own_weight, kv_index * heads_dev, heads_dev, 1)
     value_block_weight = lax.dynamic_slice_in_dim(w_value_up, kv_index * heads_dev, heads_dev, 1)
-    totals, summed = lax.psum((total_part, summed_part), ("kv", "tp"))
+    totals, summed = lax.psum(lax.psum((total_part, summed_part), "tp"), "kv")
     block_sum = lax.dynamic_slice_in_dim(summed, kv_index * heads_dev, heads_dev, 1)
     block_total = lax.dynamic_slice_in_dim(totals, kv_index * heads_dev, heads_dev, 1)
     latent_out = (block_sum + block_own[:, :, None] * new_latent_f[:, None, :]) / (

time: 342 us -> 364 us (1.064)
  waiting for transfers between devices: 89.9 us -> 127 us
  blocking collectives: 208 us -> 194 us
    psum x1 -> x2, waiting for transfers between devices: 89.8 us -> 127 us  [shards(): totals, summed = lax.psum(lax.psum((total_part, summed_part), 'tp'), 'kv')]
    psum x1 -> x2, blocking collectives: 42.7 us -> 29.1 us  [shards(): totals, summed = lax.psum(lax.psum((total_part, summed_part), 'tp'), 'kv')]
  transfers between devices with their start and end apart: 2 -> 3, of which waited for: 1 -> 2; matrix products, arithmetic and copies ran while one was open for 2% -> 2% of each run, Pallas kernels for 0% -> 0%
where the time goes in v1:
time: 364 us
  blocking collectives  194 us (53%)
  waiting for transfers between devices  127 us (35%)
  matrix products  15.6 us (4%)
  between operations  13.9 us (4%)
  local copies, waits for them, and re-layouts  8.86 us (2%)
  other arithmetic  4.22 us (1%)
    psum x2, waiting for transfers between devices, shards(): totals, summed = lax.psum(lax.psum((total_part, summed_part), 'tp'), 'kv')  127 us
    all_gather x1, blocking collectives, shards(): lax.all_gather(rope_piece[:, None], ('kv', 'tp'), axis=1, tiled=True)  41.5 us
    all_gather x1, blocking collectives, shards(): lax.all_gather(column_piece[:, None], ('kv', 'tp'), axis=1, tiled=True)  37 us
    pmax x1, blocking collectives, shards(): top_score = lax.pmax(local_top, ('kv', 'tp'))  37 us
    psum x1, blocking collectives, shards(): mixed_out = lax.psum(out_part, 'kv').astype(jnp.bfloat16)  36.4 us
    psum x2, blocking collectives, shards(): totals, summed = lax.psum(lax.psum((total_part, summed_part), 'tp'), 'kv')  29.1 us
    psum x1, blocking collectives, shards(): lax.psum((query_part, latent_part, rotary_part, square_part), 'tp')  13.4 us
  transfers between devices with their start and end apart: 3, of which 2 were waited for; matrix products, arithmetic and copies ran while one was open for 2% of the time, Pallas kernels for 0%

profile of v1, /device:TPU:0, one launch (start us, length us, event | category | flops | bytes accessed | tf_op | source)
XLA Modules:
  0.0 363.6 jit_solution(10292674910636934405)
XLA Ops:
  7.2 1.0 fusion.15
  8.2 1.5 fusion.20
  9.7 1.0 fusion.22
  10.7 1.1 fusion.24
  11.9 13.4 %all-reduce = (f32[16,4,96]{2,0,1:T(8,128)S(1)}, f32[16]{0:T(128)S(1)}, f32[16,128]{1,0:T(8,128)S(1)}, f32[16,32]{1,0:T(8,128)S(1)}) all-reduce(f32[16,4,96]{2,0,1:T(8,128)S(1)} %fusion.20, f32[16]{0:T(128)S(1)} %fusion.15, f32[16,128]{1,0:T(8,128)S(1)} %fusion.24, f32[16,32]{1,0:T(8,128)S(1)} %fusion.22), channel_id=1, replica_groups=mesh['kv'=8,'tp'=4] {'tp'}, use_global_device_ids=true, to_apply=%region_0.0 | all-reduce | flops 8720 | bytes 69760 | tf_op jit(solution)/shard_map/psum | solution.py:69
  25.3 0.1 multiply_convert_fusion.1
  25.3 1.7 fusion.1
  27.0 0.0 all-reduce.4.cloned.1.call-start
  27.1 0.7 convert_element_type.81
  27.8 0.1 broadcast_multiply_fusion
  27.8 0.1 subtract_convert_fusion.3
  28.0 0.1 slice_convert_fusion
  28.0 0.1 subtract_convert_fusion.2
  28.1 0.1 dynamic-slice_maximum_fusion
  28.2 0.1 copy.48
  28.3 41.5 %all-gather.1 = bf16[16,128,8]{0,2,1:T(8,128)(2,1)S(1)} all-gather(bf16[16,4,8]{0,2,1:T(8,128)(2,1)S(1)} %copy.48), channel_id=3, replica_groups=mesh['kv'=8,'tp'=4] {'kv','tp'}, dimensions={1}, use_global_device_ids=true | all-gather | bytes 33792 | tf_op jit(solution)/shard_map/all_gather | solution.py:88
  69.8 0.3 copy.50
  70.1 37.0 %all-gather.3 = bf16[32,32,16]{1,2,0:T(8,128)(2,1)S(1)} all-gather(bf16[1,32,16]{1,2,0:T(8,128)(2,1)S(1)} %get-tuple-element.20), channel_id=4, replica_groups=mesh['kv'=8,'tp'=4] {'kv','tp'}, dimensions={0}, use_global_device_ids=true | all-gather | bytes 33792 | tf_op jit(solution)/shard_map/all_gather | solution.py:89
  107.1 0.1 reshape.167
  107.3 0.1 fusion.54
  107.3 0.1 multiply_reduce_fusion
  107.5 0.7 broadcast_compare_fusion
  108.2 0.2 fusion.33
  108.4 0.1 bitcast_convert_fusion
  108.5 2.0 copy.75
  110.6 0.8 reshape.151
  111.3 3.7 %fusion.41 = f32[16,32,128]{2,1,0:T(8,128)S(1)} fusion(bf16[16,32,1024]{2,1,0:T(8,128)(2,1)S(1)} %reshape.151, bf16[16,128,1024]{2,1,0:T(8,128)(2,1)} %param.21), kind=kOutput, calls=%fused_computation.71 | convolution fusion | flops 134217728 | bytes 5505024 | tf_op jit(solution)/shard_map/bhr,bpr->bhp/dot_general | solution.py:110
  115.0 0.4 fusion.16
  115.4 0.3 select_reduce_fusion
  115.7 37.0 %pmax.7 = f32[16,32]{1,0:T(8,128)S(1)} all-reduce(f32[16,32]{1,0:T(8,128)S(1)} %get-tuple-element.11), channel_id=1, replica_groups=mesh['kv'=8,'tp'=4] {'kv','tp'}, use_global_device_ids=true, to_apply=%region_7.8 | all-reduce | flops 512 | bytes 4096 | tf_op jit(solution)/shard_map/pmax | solution.py:115
  152.7 2.9 fusion.9
  155.6 2.5 copy.52
  158.2 0.0 all-reduce.6.cloned.1.call-start
  158.2 53.0 %all-reduce.4.cloned.1.call-done = f32[16,32,1024]{2,0,1:T(8,128)} async-done(((f32[16,32,1024]{2,0,1:T(8,128)}), f32[16,32,1024]{2,0,1:T(8,128)}) %all-reduce.4.cloned.1.call-update) | async-done | bytes 2097168 | tf_op jit(solution)/shard_map/psum | solution.py:127
  211.2 0.7 pad_maximum_fusion
  211.9 0.7 dynamic-slice_bitcast_fusion
  212.6 2.1 constant_dynamic-slice_fusion
  214.7 0.3 fusion.7
  215.0 5.9 %psum.69 = f32[16,32]{1,0:T(8,128)S(1)} all-reduce(f32[16,32]{1,0:T(8,128)S(1)} %fusion.7), channel_id=1, replica_groups=mesh['kv'=8,'tp'=4] {'tp'}, use_global_device_ids=true, to_apply=%region_11.12 | all-reduce | flops 512 | bytes 4096 | tf_op jit(solution)/shard_map/psum | solution.py:127
  220.9 23.2 %psum.70 = f32[16,32]{1,0:T(8,128)S(1)} all-reduce(f32[16,32]{1,0:T(8,128)S(1)} %psum.69), channel_id=1, replica_groups=mesh['kv'=8,'tp'=4] {'kv'}, use_global_device_ids=true, to_apply=%region_12.13 | all-reduce | flops 512 | bytes 4096 | tf_op jit(solution)/shard_map/psum | solution.py:127
  244.1 0.1 dynamic-slice_add_fusion
  244.2 0.1 copy.53
  244.3 0.1 copy.54
  244.3 73.6 %all-reduce.6.cloned.1.call-done = f32[16,32,1024]{2,0,1:T(8,128)} async-done(((f32[16,32,1024]{2,0,1:T(8,128)}), f32[16,32,1024]{2,0,1:T(8,128)}) %all-reduce.6.cloned.1.call-update) | async-done | bytes 2097168 | tf_op jit(solution)/shard_map/psum | solution.py:127
  317.9 1.3 fusion.4
  319.2 1.3 fusion.3
  320.5 0.3 fusion.27
  320.7 36.4 %psum.71 = bf16[16,1024]{1,0:T(8,128)(2,1)} all-reduce(f32[16,1024]{1,0:T(8,128)S(1)} %fusion.27), channel_id=1, replica_groups=mesh['kv'=8,'tp'=4] {'kv'}, use_global_device_ids=true, to_apply=%region_13.14 | all-reduce | flops 16384 | bytes 98304 | tf_op jit(solution)/shard_map/psum | solution.py:135
  (18 shorter events, 0.2 us)
Async XLA Ops:
  7.2 313.3 %copy-start = (bf16[512,1024]{1,0:T(8,128)(2,1)S(1)}, bf16[512,1024]{1,0:T(8,128)(2,1)}, u32[]{:S(2)}) copy-start(bf16[512,1024]{1,0:T(8,128)(2,1)} %param.20) | copy-start | bytes 3145732
  7.2 101.2 %copy-start.2 = (f32[1024]{0:T(1024)S(1)}, f32[1024]{0:T(1024)}, u32[]{:S(2)}) copy-start(f32[1024]{0:T(1024)} %param.17) | copy-start | bytes 12292
  7.2 101.3 %all-gather.6.cloned.1.call-start = ((), (), s32[]{:S(2)}) async-start(), calls=%async_computation.2 | async-start | bytes 1081344 | tf_op jit(solution)/shard_map/all_gather | solution.py:87
  27.0 184.2 %all-reduce.4.cloned.1.call-start = ((), (), s32[]{:S(2)}) async-start(), calls=%async_computation | async-start | bytes 4194304 | tf_op jit(solution)/shard_map/psum | solution.py:127
  110.5 4.9 %copy-start.1 = (bf16[16,128,32]{1,2,0:T(8,128)(2,1)S(1)}, bf16[16,128,32]{1,2,0:T(8,128)(2,1)}, u32[]{:S(2)}) copy-start(bf16[16,128,32]{1,2,0:T(8,128)(2,1)} %param.22) | copy-start | bytes 393220
  158.2 159.7 %all-reduce.6.cloned.1.call-start = ((), (), s32[]{:S(2)}) async-start(), calls=%async_computation.1 | async-start | bytes 4194304 | tf_op jit(solution)/shard_map/psum | solution.py:127
Sparse Core Ops, SparseCore 0:
  27.1 54.0 all-gather.5
  158.3 52.8 all-reduce.3
  214.8 103.0 all-reduce.5
